TPU v7x, 512 devices: a whole 4x8x8 slice. The times are simulated.
512 devices in a mesh: sp: 64 (over z, y), tp: 8 (over x, core).
Axes of the slice: x: 4, y: 8, z: 8, core: 2. Of those that a mesh axis runs over, the one named last changes fastest.
Arguments:
- tokens: bfloat16 [16384, 2048], P('sp', 'tp'), may hold values from -24 to 24
- value_weight: bfloat16 [2, 2048, 2048], P(None, 'sp', 'tp'), may hold values from -0.125 to 0.125
- outer_weight: bfloat16 [2, 2048, 2048], P(None, 'sp', 'tp'), may hold values from -0.125 to 0.125
- inner_weight: bfloat16 [2, 2048, 2048], P(None, 'sp', 'tp'), may hold values from -0.125 to 0.125
- conv_taps: float32 [2, 3, 2048], P(None, None, 'tp'), may hold values from -3.5 to 3.5
- output_weight: bfloat16 [2, 2048, 2048], P(None, 'tp', 'sp'), may hold values from -2 to 2
- norm_gain: float32 [2, 2048], P(None, 'tp'), may hold values from 0.1 to 1.9
- norm_bias: float32 [2, 2048], P(None, 'tp'), may hold values from -3 to 3
Outputs:
- mixed_out: bfloat16 [16384, 2048], P('sp', 'tp')
All inputs are finite; a program needn't handle non-finite values.
Results may differ from a plain program's by a relative error of at most 0.03.
Values may be sent and summed in bfloat16 or wider, within the bound.
No kernel may reach another device: no remote copies, remote signals or barrier semaphores. Data moves between devices by JAX's collectives and lax.ppermute only.
A program may use at most 64 MiB of HBM per device.

v0:
```python
import functools

import jax
import jax.numpy as jnp
from jax import lax
from jax.experimental import pallas as pl
from jax.experimental.pallas import tpu as pltpu
from jax.sharding import Mesh, PartitionSpec as P


D = 2048
LAYERS = 2
TP = ("x", "core")
SP = ("z", "y")
HALO = 16
IN_UP, OUT_UP = 2.0**18, 2.0**14


def bf(x):
    return x.astype(jnp.bfloat16)


def f32(x):
    return x.astype(jnp.float32)


HBM = pl.BlockSpec(memory_space=pltpu.HBM)
VMEM = pl.BlockSpec(memory_space=pltpu.VMEM)


def pack_kernel(value, outer, inner, out_t, tokens, gain, bias, early, late, copies, held, rows, left, sems):
    fills = [pltpu.make_async_copy(w, held.at[i], sems.at[i]) for i, w in enumerate((value, outer, inner, out_t))]
    fills.append(pltpu.make_async_copy(gain, left.at[0:2], sems.at[4]))
    fills.append(pltpu.make_async_copy(bias, left.at[2:4], sems.at[5]))
    fills.append(pltpu.make_async_copy(tokens, rows.at[0:256], sems.at[6]))
    for copy in fills[4:] + fills[:4]:
        copy.start()
    fills[4].wait()
    fills[5].wait()
    rest = left[...]
    terms = []
    for _ in range(3):
        terms.append(f32(bf(rest)))
        rest = rest - terms[-1]
    terms.append(jnp.zeros_like(rest))
    rows[256:] = bf(jnp.concatenate(terms, axis=0))
    fills[6].wait()
    sends = [pltpu.make_async_copy(rows, copies.at[i, HALO : HALO + 272], sems.at[7 + i]) for i in range(8)]
    for copy in sends:
        copy.start()
    for i in range(4):
        at = slice(256 * i, 256 * (i + 1))
        fills[i].wait()
        early[:, at] = bf(f32(held[i, 0]) * (IN_UP if i < 3 else OUT_UP))
        late[:, at] = held[i, 1]
    for copy in sends:
        copy.wait()


HBM = pl.BlockSpec(memory_space=pltpu.HBM)
VMEM = pl.BlockSpec(memory_space=pltpu.VMEM)


def pack(value, outer, inner, out_t, tokens, gain, bias):
    shape = jax.ShapeDtypeStruct((32, 1024), jnp.bfloat16)
    return pl.pallas_call(
        pack_kernel,
        in_specs=[HBM] * 7,
        out_specs=(VMEM, VMEM, HBM),
        out_shape=(shape, shape, jax.ShapeDtypeStruct((8, 288, 256), jnp.bfloat16)),
        scratch_shapes=[
            pltpu.VMEM((4, 2, 32, 256), jnp.bfloat16),
            pltpu.VMEM((272, 256), jnp.bfloat16),
            pltpu.VMEM((4, 256), jnp.float32),
            pltpu.SemaphoreType.DMA((15,)),
        ],
        cost_estimate=pl.CostEstimate(flops=2000000, bytes_accessed=1700000, transcendentals=0),
    )(value, outer, inner, out_t, tokens, gain, bias)


def norm(pre, gain, bias):
    mean = jnp.mean(pre, axis=-1, keepdims=True)
    cent = pre - mean
    var = jnp.mean(cent * cent, axis=-1, keepdims=True)
    return bf(cent * lax.rsqrt(var + 1e-05) * gain + bias)


def shards(tokens, value, outer, inner, taps, out, gain, bias):
    taps = jnp.swapaxes(taps, 0, 1)
    halo = lax.ppermute(tokens[-HALO:], SP, [(i, i + 1) for i in range(63)])
    early, late, copies = pack(value, outer, inner, jnp.swapaxes(out, 1, 2), tokens, gain, bias)
    late = lax.all_gather(late, SP, axis=0, tiled=True)
    copies = lax.dynamic_update_slice(copies, jnp.broadcast_to(halo[None], (8, HALO, 256)), (0, 0, 0))
    everyone = lax.all_to_all(copies, TP, 0, 0, tiled=True)
    early = lax.all_gather(early.astype(jnp.float16), SP, axis=0, tiled=True)

    weights = [bf(early[:, 256 * i : 256 * (i + 1)]) for i in range(4)]
    sent, half = front(everyone, weights, taps)
    got = lax.ppermute(sent, "core", [(0, 1), (1, 0)])
    mine, kept, table = aside(half, weights[3], everyone)
    got = lax.all_to_all(folded(got, mine), "x", 0, 0, tiled=True)
    own, before = middle(got, kept, table)
    every = lax.all_gather(own.astype(jnp.float16), TP, axis=0, tiled=True)

    sent, half = rear(bf(every), before, late, taps)
    got = lax.ppermute(sent, "core", [(0, 1), (1, 0)])
    mine = own_product(half, late, 768, 1.0, 52)
    got = lax.all_to_all(bf(f32(got) + f32(mine)).reshape(4, 32, D), "x", 0, 0, tiled=True)
    return lax.all_to_all(last(got, own, table), TP, 0, 0, tiled=True).reshape(256, 256)


def out_product(rows, w_out, down, target):
    for n in range(4):
        at = slice(512 * n, 512 * (n + 1))
        part = lax.dot_general(rows, w_out[at], (((1,), (1,)), ((), ())), preferred_element_type=jnp.float32)
        target[:, at] = bf(part * down)


def front_kernel(xs, w_u, w_outer, w_inner, w_out, taps, sent, own, x, g, half, held, parts, sems):
    core = lax.axis_index("core")
    first = jnp.logical_and(lax.axis_index("z") == 0, lax.axis_index("y") == 0)
    rows = HALO + 256
    blocks = [
        pltpu.make_async_copy(xs.at[4 * i : 4 * (i + 1), 0:rows], parts.at[4 * i : 4 * (i + 1)], sems.at[i])
        for i in range(2)
    ]
    weight = pltpu.make_async_copy(w_out, held, sems.at[2])
    for copy in blocks:
        copy.start()
    sums = [0.0, 0.0, 0.0]
    for part in range(2):
        blocks[part].wait()
        if part == 1:
            weight.start()
        for j in range(4 * part, 4 * (part + 1)):
            x[:, 256 * j : 256 * (j + 1)] = parts[j]
        at = slice(1024 * part, 1024 * (part + 1))
        for i, w in enumerate((w_u, w_outer, w_inner)):
            sums[i] = sums[i] + jnp.dot(x[:, at], w[at], preferred_element_type=jnp.float32)
    u, outer, inner = (f32(bf(total * (1.0 / IN_UP))) for total in sums)
    row = lax.broadcasted_iota(jnp.int32, u.shape, 0)
    z = jnp.where(jnp.logical_and(first, row < HALO), 0.0, inner * u)
    conv = taps[2, 0:1] * z + taps[1, 0:1] * pltpu.roll(z, 1, 0) + taps[0, 0:1] * pltpu.roll(z, 2, 0)
    g[...] = bf(outer * conv)
    for target, which in ((half, 1 - core), (own, core)):
        target[128:] = g[HALO - 8 : HALO]
        for i in range(4):
            target[32 * i : 32 * (i + 1)] = g[pl.ds(pl.multiple_of(HALO + 64 * i + 32 * which, 16), 32)]
    weight.wait()
    out_product(half[...], held, 1.0 / OUT_UP, sent)


def front(xs, weights, taps):
    shape = jax.ShapeDtypeStruct
    return pl.pallas_call(
        front_kernel,
        in_specs=[HBM, VMEM, VMEM, VMEM, HBM, VMEM],
        out_specs=(VMEM,) * 2,
        out_shape=(shape((136, D), jnp.bfloat16), shape((136, 256), jnp.bfloat16)),
        scratch_shapes=[
            pltpu.VMEM((HALO + 256, D), jnp.bfloat16),
            pltpu.VMEM((HALO + 256, 256), jnp.bfloat16),
            pltpu.VMEM((136, 256), jnp.bfloat16),
            pltpu.VMEM((D, 256), jnp.bfloat16),
            pltpu.VMEM((8, HALO + 256, 256), jnp.bfloat16),
            pltpu.SemaphoreType.DMA((3,)),
        ],
        compiler_params=pltpu.CompilerParams(vmem_limit_bytes=50 * 2**20),
        cost_estimate=pl.CostEstimate(flops=1200000000, bytes_accessed=7000000, transcendentals=0),
    )(xs, *weights, taps)


def aside_kernel(rows, w, xs, mine, kept, table, held, x, tails, sems):
    tp = 2 * lax.axis_index("x") + lax.axis_index("core")
    weight = pltpu.make_async_copy(w, held, sems.at[0])
    weight.start()
    start = pl.multiple_of(HALO + 32 * tp, 16)
    copies = [
        pltpu.make_async_copy(xs.at[:, pl.ds(start, 32)], x.at[:, 0:32], sems.at[1]),
        pltpu.make_async_copy(xs.at[:, HALO - 8 : HALO], x.at[:, 32:40], sems.at[2]),
        pltpu.make_async_copy(xs.at[:, HALO + 256 : HALO + 272], tails, sems.at[3]),
    ]
    for copy in copies:
        copy.start()
    weight.wait()
    out_product(rows[...], held, 1.0 / OUT_UP, mine)
    for copy in copies:
        copy.wait()
    for j in range(8):
        at = slice(256 * j, 256 * (j + 1))
        kept[:, at] = (2.0 * LAYERS) ** 0.25 * f32(x[j])
        tail = f32(tails[j])
        table[:, at] = tail[0:4] + tail[4:8] + tail[8:12]


def aside(rows, w, xs):
    shape = jax.ShapeDtypeStruct
    return pl.pallas_call(
        aside_kernel,
        in_specs=[VMEM, HBM, HBM],
        out_specs=(VMEM,) * 3,
        out_shape=(shape((136, D), jnp.bfloat16), shape((40, D), jnp.float32), shape((4, D), jnp.float32)),
        scratch_shapes=[
            pltpu.VMEM((D, 256), jnp.bfloat16),
            pltpu.VMEM((8, 40, 256), jnp.bfloat16),
            pltpu.VMEM((8, 16, 256), jnp.bfloat16),
            pltpu.SemaphoreType.DMA((4,)),
        ],
        compiler_params=pltpu.CompilerParams(vmem_limit_bytes=52 * 2**20),
        cost_estimate=pl.CostEstimate(flops=800000000, bytes_accessed=2000000, transcendentals=0),
    )(rows, w, xs)


def own_kernel(column, down, rows, w, mine, held, sems):
    copies = [
        pltpu.make_async_copy(w.at[at, column : column + 256], held.at[at], sems.at[i])
        for i, at in enumerate(pl.ds(512 * i, 512) for i in range(4))
    ]
    for copy in copies:
        copy.start()
    for i in range(4):
        copies[i].wait()
        at = slice(512 * i, 512 * (i + 1))
        part = lax.dot_general(rows[...], held[at], (((1,), (1,)), ((), ())), preferred_element_type=jnp.float32)
        mine[:, at] = bf(part * down)


def own_product(rows, w, column, down, limit):
    return pl.pallas_call(
        functools.partial(own_kernel, column, down),
        in_specs=[VMEM, HBM],
        out_specs=VMEM,
        out_shape=jax.ShapeDtypeStruct((rows.shape[0], D), jnp.bfloat16),
        scratch_shapes=[pltpu.VMEM((D, 256), jnp.bfloat16), pltpu.SemaphoreType.DMA((4,))],
        compiler_params=pltpu.CompilerParams(vmem_limit_bytes=limit * 2**20),
        cost_estimate=pl.CostEstimate(flops=800000000, bytes_accessed=2000000, transcendentals=0),
    )(rows, w)


def fold_kernel(got, mine, out, strip):
    total = f32(got[...]) + f32(mine[...])
    for i in range(4):
        out[i, :, :D] = bf(total[32 * i : 32 * (i + 1)])
    for t in range(2):
        for r in range(16):
            strip[16 * t + r : 16 * t + r + 1] = total[134 + t : 135 + t, 128 * r : 128 * (r + 1)]
    for i in range(4):
        out[i, :, D:] = bf(strip[...])


def folded(got, mine):
    return pl.pallas_call(
        fold_kernel,
        out_shape=jax.ShapeDtypeStruct((4, 32, D + 128), jnp.bfloat16),
        scratch_shapes=[pltpu.VMEM((32, 128), jnp.float32)],
        compiler_params=pltpu.CompilerParams(vmem_limit_bytes=6 * 2**20),
        cost_estimate=pl.CostEstimate(flops=1000000, bytes_accessed=2200000, transcendentals=0),
    )(got, mine)


def middle_kernel(got, kept, table, own, before, wide):
    total = f32(got[0]) + f32(got[1]) + f32(got[2]) + f32(got[3])
    wide[...] = jnp.zeros_like(wide)
    for t in range(2):
        for r in range(16):
            wide[6 + t : 7 + t, 128 * r : 128 * (r + 1)] = total[16 * t + r : 16 * t + r + 1, D:]
    gain, bias = table[0:1], table[2:3]
    own[...] = norm(kept[:32] + total[:, :D], gain, bias)
    before[...] = norm(kept[32:] + wide[...], gain, bias)


def middle(got, kept, table):
    shape = jax.ShapeDtypeStruct
    return pl.pallas_call(
        middle_kernel,
        out_shape=(shape((32, D), jnp.bfloat16), shape((8, D), jnp.bfloat16)),
        scratch_shapes=[pltpu.VMEM((8, D), jnp.float32)],
        compiler_params=pltpu.CompilerParams(vmem_limit_bytes=6 * 2**20),
        cost_estimate=pl.CostEstimate(flops=2000000, bytes_accessed=1200000, transcendentals=100),
    )(got, kept, table)


def rear_kernel(x, before, w, taps, sent, own, held, acc, g, half, sems):
    core = lax.axis_index("core")
    first = jnp.logical_and(lax.axis_index("z") == 0, lax.axis_index("y") == 0)
    step = D // 4
    copies = [
        pltpu.make_async_copy(w.at[at, 0:768], held.at[at, 0:768], sems.at[i])
        for i, at in enumerate(pl.ds(step * i, step) for i in range(4))
    ]
    copies.append(pltpu.make_async_copy(w.at[:, 768:1024], held.at[:, 768:1024], sems.at[4]))
    for copy in copies:
        copy.start()
    for i in range(4):
        copies[i].wait()
        at = slice(step * i, step * (i + 1))
        for rows, source in ((slice(0, 8), before), (slice(8, 264), x)):
            part = jnp.dot(source[:, at], held[at, :768], preferred_element_type=jnp.float32)
            acc[rows] = part if i == 0 else acc[rows] + part
    u, outer, inner = (f32(bf(acc[:, 256 * i : 256 * (i + 1)])) for i in range(3))
    row = lax.broadcasted_iota(jnp.int32, u.shape, 0)
    z = jnp.where(jnp.logical_and(first, row < 8), 0.0, inner * u)
    conv = taps[2, 1:2] * z + taps[1, 1:2] * pltpu.roll(z, 1, 0) + taps[0, 1:2] * pltpu.roll(z, 2, 0)
    g[...] = bf((outer * conv)[8:])
    for target, which in ((half, 1 - core), (own, core)):
        for i in range(4):
            target[32 * i : 32 * (i + 1)] = g[pl.ds(pl.multiple_of(64 * i + 32 * which, 16), 32)]
    copies[4].wait()
    out_product(half[...], held.at[:, 768:1024], 1.0, sent)


def rear(x, before, w, taps):
    shape = jax.ShapeDtypeStruct
    return pl.pallas_call(
        rear_kernel,
        in_specs=[VMEM, VMEM, HBM, VMEM],
        out_specs=(VMEM, VMEM),
        out_shape=(shape((128, D), jnp.bfloat16), shape((128, 256), jnp.bfloat16)),
        scratch_shapes=[
            pltpu.VMEM((D, 1024), jnp.bfloat16),
            pltpu.VMEM((264, 768), jnp.float32),
            pltpu.VMEM((256, 256), jnp.bfloat16),
            pltpu.VMEM((128, 256), jnp.bfloat16),
            pltpu.SemaphoreType.DMA((5,)),
        ],
        compiler_params=pltpu.CompilerParams(vmem_limit_bytes=50 * 2**20),
        cost_estimate=pl.CostEstimate(flops=1200000000, bytes_accessed=7000000, transcendentals=0),
    )(x, before, w, taps)


def last_kernel(got, own, table, out):
    total = f32(got[0]) + f32(got[1]) + f32(got[2]) + f32(got[3])
    alpha = (2.0 * LAYERS) ** 0.25
    state = norm(alpha * f32(own[...]) + total, table[1:2], table[3:4])
    for i in range(8):
        out[i] = state[:, 256 * i : 256 * (i + 1)]


def last(got, own, table):
    return pl.pallas_call(
        last_kernel,
        out_shape=jax.ShapeDtypeStruct((8, 32, 256), jnp.bfloat16),
        compiler_params=pltpu.CompilerParams(vmem_limit_bytes=6 * 2**20),
        cost_estimate=pl.CostEstimate(flops=2000000, bytes_accessed=1200000, transcendentals=100),
    )(got, own, table)


def solution(mesh):
    mesh = Mesh(mesh.devices.reshape(8, 8, 4, 2), ("z", "y", "x", "core"))
    in_specs = (
        P(SP, TP),
        P(None, SP, TP),
        P(None, SP, TP),
        P(None, SP, TP),
        P(None, None, TP),
        P(None, TP, SP),
        P(None, TP),
        P(None, TP),
    )
    return jax.shard_map(shards, mesh=mesh, in_specs=in_specs, out_specs=P(SP, TP), check_vma=False)
```

profile of v0, /device:TPU:1, one launch (start us, length us, event | category | flops | bytes accessed | tf_op | source)
XLA Modules:
  0.0 164.2 jit_solution(10336949002557334536)
XLA Ops:
  6.5 0.0 all-gather.4.cloned.1.call-start
  6.5 2.7 %shard_map.82 = (bf16[32,1024]{1,0:T(8,128)(2,1)}, bf16[32,1024]{1,0:T(8,128)(2,1)}, bf16[8,288,256]{2,1,0:T(8,128)(2,1)}) custom-call(bf16[2,32,256]{2,1,0:T(8,128)(2,1)} %value.1, bf16[2,32,256]{2,1,0:T(8,128)(2,1)} %outer.1, bf16[2,32,256]{2,1,0:T(8,128)(2,1)} %inner.1, bf16[2,32,256]{2,1,0:T(8,128)(2,1)} %bitcast.8, bf16[256,256]{1,0:T(8,128)(2,1)} %tokens.1, ...), custom_call_target="tpu_custom_call" | custom-call | flops 2000000 | bytes 1700000 | tf_op jit(solution)/shard_map/pallas_call | solution.py:66
  9.2 0.0 all-gather.4.cloned.1.call-update
  9.3 0.7 slice.15
  10.0 4.0 %collective-permute-start = (bf16[16,256]{1,0:T(8,128)(2,1)S(1)}, bf16[16,256]{1,0:T(8,128)(2,1)S(1)}, u32[]{:S(2)}, u32[]{:S(2)}) collective-permute-start(bf16[16,256]{1,0:T(8,128)(2,1)S(1)} %slice.15), channel_id=1, source_target_pairs={{0,8},{8,16},{16,24},{24,32},{32,40},{40,48},{48,56},{56,64},{64,7... | collective-permute-start | bytes 24584 | tf_op jit(solution)/shard_map/ppermute | solution.py:90
  14.0 0.9 convert_element_type.30
  14.8 0.0 collective-permute-done
  14.8 0.6 broadcast_dynamic-update-slice_fusion
  15.5 8.7 %all-to-all-start = ((bf16[8,288,256]{2,1,0:T(8,128)(2,1)}), bf16[8,288,256]{2,1,0:T(8,128)(2,1)}, u32[]{:S(2)}, u32[]{:S(2)}) async-start(bf16[8,288,256]{2,1,0:T(8,128)(2,1)} %broadcast_dynamic-update-slice_fusion), calls=%async_computation | async-start | bytes 2359296 | tf_op jit(solution)/shard_map/all_to_all | solution.py:94
  24.2 55.5 %all-gather.5 = f16[2048,1024]{1,0:T(8,128)(2,1)S(1)} all-gather(f16[32,1024]{1,0:T(8,128)(2,1)S(1)} %convert_element_type.30), channel_id=1, replica_groups=mesh['z'=8,'y'=8,'x'=4,'core'=2] {'z','y'}, dimensions={0}, use_global_device_ids=true | all-gather | bytes 4259840 | tf_op jit(solution)/shard_map/all_gather | solution.py:95
  79.7 1.6 slice_convert_fusion
  81.3 0.0 all-to-all-done.xs
  81.3 0.0 copy-done
  81.3 3.4 %shard_map.83 = (bf16[136,2048]{1,0:T(8,128)(2,1)S(1)}, bf16[136,256]{1,0:T(8,128)(2,1)S(1)}) custom-call(bf16[8,288,256]{2,1,0:T(8,128)(2,1)} %all-to-all-done.xs, bf16[2048,256]{1,0:T(8,128)(2,1)S(1)} %get-tuple-element.32.w_u, bf16[2048,256]{1,0:T(8,128)(2,1)S(1)} %get-tuple-element.31.w_outer, bf16[2048,256]{1,0:T(8,128)(2,1)S(1)} %get-tuple-element.30.w_inner, ...), custom_call_target="tpu_custom_call" | custom-call | flops 1200000000 | bytes 7000000 | tf_op jit(solution)/shard_map/pallas_call | solution.py:155
  84.7 10.6 %collective-permute-start.1 = (bf16[136,2048]{1,0:T(8,128)(2,1)S(1)}, bf16[136,2048]{1,0:T(8,128)(2,1)S(1)}, u32[]{:S(2)}, u32[]{:S(2)}) collective-permute-start(bf16[136,2048]{1,0:T(8,128)(2,1)S(1)} %get-tuple-element.19), channel_id=1, source_target_pairs={{0,1},{1,0},{2,3},{3,2},{4,5},{5,4},{6,7},{7,6},{8,9},{9,8},{10,11... | collective-permute-start | bytes 1671176 | tf_op jit(solution)/shard_map/ppermute | solution.py:99
  95.3 1.8 %shard_map.84 = (bf16[136,2048]{1,0:T(8,128)(2,1)S(1)}, f32[40,2048]{1,0:T(8,128)S(1)}, f32[4,2048]{1,0:T(4,128)S(1)}) custom-call(bf16[136,256]{1,0:T(8,128)(2,1)S(1)} %get-tuple-element.20.rows, bf16[2048,256]{1,0:T(8,128)(2,1)} %get-tuple-element.29.w_out.w, bf16[8,288,256]{2,1,0:T(8,128)(2,1)} %all-to-all-done.xs), custom_call_target="tpu_custom_call" | custom-call | flops 800000000 | bytes 2000000 | tf_op jit(solution)/shard_map/pallas_call | solution.py:198
  97.1 0.0 collective-permute-done.1.got
  97.1 0.3 shard_map.85
  97.4 15.4 %all_to_all.20.got = bf16[4,32,2176]{2,1,0:T(8,128)(2,1)S(1)} all-to-all(bf16[4,32,2176]{2,1,0:T(8,128)(2,1)S(1)} %shard_map.85), channel_id=1, replica_groups=mesh['z'=8,'y'=8,'x'=4,'core'=2] {'x'}, dimensions={0} | all-to-all | bytes 1114112 | tf_op jit(solution)/shard_map/all_to_all | solution.py:101
  112.8 0.3 shard_map.86
  113.1 15.0 %all-gather.6 = f16[256,2048]{1,0:T(8,128)(2,1)S(1)} all-gather(f16[32,2048]{1,0:T(8,128)(2,1)S(1)} %convert_element_type.35), channel_id=1, replica_groups=mesh['z'=8,'y'=8,'x'=4,'core'=2] {'x','core'}, dimensions={0}, use_global_device_ids=true | all-gather | bytes 1179648 | tf_op jit(solution)/shard_map/all_gather | solution.py:103
  128.2 0.1 convert_element_type.36.x
  128.3 0.0 all-gather.4.cloned.1.call-done.w
  128.3 3.5 %shard_map.87 = (bf16[128,2048]{1,0:T(8,128)(2,1)S(1)}, bf16[128,256]{1,0:T(8,128)(2,1)S(1)}) custom-call(bf16[256,2048]{1,0:T(8,128)(2,1)S(1)} %convert_element_type.36.x, bf16[8,2048]{1,0:T(8,128)(2,1)S(1)} %get-tuple-element.25.before, bf16[2048,1024]{1,0:T(8,128)(2,1)} %all-gather.4.cloned.1.call-done.w, f32[3,2,256]{2,1,0:T(2,128)S(1)} %bitcast.5), custom_call_target="tpu_custom_call" | custom-call | flops 1200000000 | bytes 7000000 | tf_op jit(solution)/shard_map/pallas_call | solution.py:314
  131.8 2.1 %collective-permute-start.2 = (bf16[128,2048]{1,0:T(8,128)(2,1)S(1)}, bf16[128,2048]{1,0:T(8,128)(2,1)S(1)}, u32[]{:S(2)}, u32[]{:S(2)}) collective-permute-start(bf16[128,2048]{1,0:T(8,128)(2,1)S(1)} %get-tuple-element.27), channel_id=1, source_target_pairs={{0,1},{1,0},{2,3},{3,2},{4,5},{5,4},{6,7},{7,6},{8,9},{9,8},{10,11... | collective-permute-start | bytes 1572872 | tf_op jit(solution)/shard_map/ppermute | solution.py:106
  133.9 1.9 %shard_map.88 = bf16[128,2048]{1,0:T(8,128)(2,1)S(1)} custom-call(bf16[128,256]{1,0:T(8,128)(2,1)S(1)} %get-tuple-element.28.rows, bf16[2048,1024]{1,0:T(8,128)(2,1)} %all-gather.4.cloned.1.call-done.w), custom_call_target="tpu_custom_call" | custom-call | flops 800000000 | bytes 2000000 | tf_op jit(solution)/shard_map/pallas_call | solution.py:229
  135.8 0.0 collective-permute-done.2
  135.8 0.1 add_convert_fusion
  136.0 11.5 %all_to_all.21.got = bf16[4,32,2048]{2,1,0:T(8,128)(2,1)S(1)} all-to-all(bf16[4,32,2048]{2,1,0:T(8,128)(2,1)S(1)} %bitcast.6), channel_id=1, replica_groups=mesh['z'=8,'y'=8,'x'=4,'core'=2] {'x'}, dimensions={0} | all-to-all | bytes 1048576 | tf_op jit(solution)/shard_map/all_to_all | solution.py:108
  147.4 0.3 shard_map.89
  147.7 9.0 %all_to_all.22 = bf16[8,32,256]{2,1,0:T(8,128)(2,1)S(1)} all-to-all(bf16[8,32,256]{2,1,0:T(8,128)(2,1)S(1)} %shard_map.89), channel_id=1, replica_groups=mesh['z'=8,'y'=8,'x'=4,'core'=2] {'x','core'}, dimensions={0} | all-to-all | bytes 262144 | tf_op jit(solution)/shard_map/all_to_all | solution.py:109
  156.7 0.7 copy.11
  (2 shorter events, 0.0 us)
Async XLA Ops:
  6.5 121.8 %all-gather.4.cloned.1.call-start = ((), (), s32[]{:S(2)}) async-start(), calls=%async_computation.4 | async-start | bytes 4259840 | tf_op jit(solution)/shard_map/all_gather | solution.py:92
  10.0 4.9 %collective-permute-start = (bf16[16,256]{1,0:T(8,128)(2,1)S(1)}, bf16[16,256]{1,0:T(8,128)(2,1)S(1)}, u32[]{:S(2)}, u32[]{:S(2)}) collective-permute-start(bf16[16,256]{1,0:T(8,128)(2,1)S(1)} %slice.15), channel_id=1, source_target_pairs={{0,8},{8,16},{16,24},{24,32},{32,40},{40,48},{48,56},{56,64},{64,7... | collective-permute-start | bytes 24584 | tf_op jit(solution)/shard_map/ppermute | solution.py:90
  15.5 65.8 %all-to-all-start = ((bf16[8,288,256]{2,1,0:T(8,128)(2,1)}), bf16[8,288,256]{2,1,0:T(8,128)(2,1)}, u32[]{:S(2)}, u32[]{:S(2)}) async-start(bf16[8,288,256]{2,1,0:T(8,128)(2,1)} %broadcast_dynamic-update-slice_fusion), calls=%async_computation | async-start | bytes 2359296 | tf_op jit(solution)/shard_map/all_to_all | solution.py:94
  79.7 1.6 %copy-start = (f32[2,3,256]{2,0,1:T(2,128)S(1)}, f32[2,3,256]{2,0,1:T(2,128)}, u32[]{:S(2)}) copy-start(f32[2,3,256]{2,0,1:T(2,128)} %param.12) | copy-start | bytes 18436
  84.7 12.4 %collective-permute-start.1 = (bf16[136,2048]{1,0:T(8,128)(2,1)S(1)}, bf16[136,2048]{1,0:T(8,128)(2,1)S(1)}, u32[]{:S(2)}, u32[]{:S(2)}) collective-permute-start(bf16[136,2048]{1,0:T(8,128)(2,1)S(1)} %get-tuple-element.19), channel_id=1, source_target_pairs={{0,1},{1,0},{2,3},{3,2},{4,5},{5,4},{6,7},{7,6},{8,9},{9,8},{10,11... | collective-permute-start | bytes 1671176 | tf_op jit(solution)/shard_map/ppermute | solution.py:99
  131.8 4.0 %collective-permute-start.2 = (bf16[128,2048]{1,0:T(8,128)(2,1)S(1)}, bf16[128,2048]{1,0:T(8,128)(2,1)S(1)}, u32[]{:S(2)}, u32[]{:S(2)}) collective-permute-start(bf16[128,2048]{1,0:T(8,128)(2,1)S(1)} %get-tuple-element.27), channel_id=1, source_target_pairs={{0,1},{1,0},{2,3},{3,2},{4,5},{5,4},{6,7},{7,6},{8,9},{9,8},{10,11... | collective-permute-start | bytes 1572872 | tf_op jit(solution)/shard_map/ppermute | solution.py:106
Sparse Core Ops, SparseCore 0:
  10.4 91.4 all-gather.3
where the time goes:
time: 165 us; the launch traced here: 164 us
  blocking collectives  106 us (64%)
  starting transfers between devices  25.4 us (15%)
  Pallas kernels  14.2 us (9%)
  between operations  13.5 us (8%)
  other arithmetic  2.78 us (2%)
  local copies, waits for them, and re-layouts  2 us (1%)
    all_gather x1, blocking collectives, shards(): early = lax.all_gather(early.astype(jnp.float16), SP, axis=0, tiled=True)  55.5 us
    all_to_all x1, blocking collectives, shards(): got = lax.all_to_all(folded(got, mine), 'x', 0, 0, tiled=True)  15.4 us
    all_gather x1, blocking collectives, shards(): every = lax.all_gather(own.astype(jnp.float16), TP, axis=0, tiled=True)  15 us
    ppermute x2, starting transfers between devices, shards(): got = lax.ppermute(sent, 'core', [(0, 1), (1, 0)])  12.6 us
    all_to_all x1, blocking collectives, shards(): lax.all_to_all(bf(f32(got) + f32(mine)).reshape(4, 32, D), 'x', 0, 0, til...  11.5 us
    all_to_all x1, blocking collectives, shards(): lax.all_to_all(last(got, own, table), TP, 0, 0, tiled=True)  8.97 us
    all_to_all x1, starting transfers between devices, shards(): everyone = lax.all_to_all(copies, TP, 0, 0, tiled=True)  8.74 us
    ppermute x1, starting transfers between devices, shards(): halo = lax.ppermute(tokens[-HALO:], SP, [(i, i + 1) for i in range(63)])  4.01 us
  transfers between devices with their start and end apart: 5, of which 0 were waited for; matrix products, arithmetic and copies ran while one was open for 2% of the time, Pallas kernels for 5%

commit v1 on v0

--- a/solution.py
+++ b/solution.py
@@ -130,7 +130,7 @@
     sums = [0.0, 0.0, 0.0]
     for part in range(2):
         blocks[part].wait()
-        if part == 1:
+        if part == 0:
             weight.start()
         for j in range(4 * part, 4 * (part + 1)):
             x[:, 256 * j : 256 * (j + 1)] = parts[j]
@@ -211,18 +211,11 @@
     )(rows, w, xs)
 
 
-def own_kernel(column, down, rows, w, mine, held, sems):
-    copies = [
-        pltpu.make_async_copy(w.at[at, column : column + 256], held.at[at], sems.at[i])
-        for i, at in enumerate(pl.ds(512 * i, 512) for i in range(4))
-    ]
-    for copy in copies:
-        copy.start()
-    for i in range(4):
-        copies[i].wait()
-        at = slice(512 * i, 512 * (i + 1))
-        part = lax.dot_general(rows[...], held[at], (((1,), (1,)), ((), ())), preferred_element_type=jnp.float32)
-        mine[:, at] = bf(part * down)
+def own_kernel(column, down, rows, w, mine, held, sem):
+    copy = pltpu.make_async_copy(w.at[:, column : column + 256], held, sem.at[0])
+    copy.start()
+    copy.wait()
+    out_product(rows[...], held, down, mine)
 
 
 def own_product(rows, w, column, down, limit):
@@ -231,7 +224,7 @@
         in_specs=[VMEM, HBM],
         out_specs=VMEM,
         out_shape=jax.ShapeDtypeStruct((rows.shape[0], D), jnp.bfloat16),
-        scratch_shapes=[pltpu.VMEM((D, 256), jnp.bfloat16), pltpu.SemaphoreType.DMA((4,))],
+        scratch_shapes=[pltpu.VMEM((D, 256), jnp.bfloat16), pltpu.SemaphoreType.DMA((1,))],
         compiler_params=pltpu.CompilerParams(vmem_limit_bytes=limit * 2**20),
         cost_estimate=pl.CostEstimate(flops=800000000, bytes_accessed=2000000, transcendentals=0),
     )(rows, w)

time: 165 us -> 165 us (level)
  no operation moved by 1% of the time
where the time goes in v1:
time: 165 us; the launch traced here: 164 us
  blocking collectives  106 us (64%)
  starting transfers between devices  25.4 us (15%)
  Pallas kernels  14 us (8%)
  between operations  13.5 us (8%)
  other arithmetic  2.78 us (2%)
  local copies, waits for them, and re-layouts  2 us (1%)
    all_gather x1, blocking collectives, shards(): early = lax.all_gather(early.astype(jnp.float16), SP, axis=0, tiled=True)  55.5 us
    all_to_all x1, blocking collectives, shards(): got = lax.all_to_all(folded(got, mine), 'x', 0, 0, tiled=True)  15.4 us
    all_gather x1, blocking collectives, shards(): every = lax.all_gather(own.astype(jnp.float16), TP, axis=0, tiled=True)  15 us
    ppermute x2, starting transfers between devices, shards(): got = lax.ppermute(sent, 'core', [(0, 1), (1, 0)])  12.6 us
    all_to_all x1, blocking collectives, shards(): lax.all_to_all(bf(f32(got) + f32(mine)).reshape(4, 32, D), 'x', 0, 0, til...  11.5 us
    all_to_all x1, blocking collectives, shards(): lax.all_to_all(last(got, own, table), TP, 0, 0, tiled=True)  8.97 us
    all_to_all x1, starting transfers between devices, shards(): everyone = lax.all_to_all(copies, TP, 0, 0, tiled=True)  8.74 us
    ppermute x1, starting transfers between devices, shards(): halo = lax.ppermute(tokens[-HALO:], SP, [(i, i + 1) for i in range(63)])  4.01 us
  transfers between devices with their start and end apart: 5, of which 0 were waited for; matrix products, arithmetic and copies ran while one was open for 2% of the time, Pallas kernels for 5%

profile of v1, /device:TPU:1, one launch (start us, length us, event | category | flops | bytes accessed | tf_op | source)
XLA Modules:
  0.0 164.0 jit_solution(15436824125647484979)
XLA Ops:
  6.5 0.0 all-gather.4.cloned.1.call-start
  6.5 2.7 %shard_map.82 = (bf16[32,1024]{1,0:T(8,128)(2,1)}, bf16[32,1024]{1,0:T(8,128)(2,1)}, bf16[8,288,256]{2,1,0:T(8,128)(2,1)}) custom-call(bf16[2,32,256]{2,1,0:T(8,128)(2,1)} %value.1, bf16[2,32,256]{2,1,0:T(8,128)(2,1)} %outer.1, bf16[2,32,256]{2,1,0:T(8,128)(2,1)} %inner.1, bf16[2,32,256]{2,1,0:T(8,128)(2,1)} %bitcast.8, bf16[256,256]{1,0:T(8,128)(2,1)} %tokens.1, ...), custom_call_target="tpu_custom_call" | custom-call | flops 2000000 | bytes 1700000 | tf_op jit(solution)/shard_map/pallas_call | solution.py:66
  9.2 0.0 all-gather.4.cloned.1.call-update
  9.3 0.7 slice.15
  10.0 4.0 %collective-permute-start = (bf16[16,256]{1,0:T(8,128)(2,1)S(1)}, bf16[16,256]{1,0:T(8,128)(2,1)S(1)}, u32[]{:S(2)}, u32[]{:S(2)}) collective-permute-start(bf16[16,256]{1,0:T(8,128)(2,1)S(1)} %slice.15), channel_id=1, source_target_pairs={{0,8},{8,16},{16,24},{24,32},{32,40},{40,48},{48,56},{56,64},{64,7... | collective-permute-start | bytes 24584 | tf_op jit(solution)/shard_map/ppermute | solution.py:90
  14.0 0.9 convert_element_type.30
  14.8 0.0 collective-permute-done
  14.8 0.6 broadcast_dynamic-update-slice_fusion
  15.5 8.7 %all-to-all-start = ((bf16[8,288,256]{2,1,0:T(8,128)(2,1)}), bf16[8,288,256]{2,1,0:T(8,128)(2,1)}, u32[]{:S(2)}, u32[]{:S(2)}) async-start(bf16[8,288,256]{2,1,0:T(8,128)(2,1)} %broadcast_dynamic-update-slice_fusion), calls=%async_computation | async-start | bytes 2359296 | tf_op jit(solution)/shard_map/all_to_all | solution.py:94
  24.2 55.5 %all-gather.5 = f16[2048,1024]{1,0:T(8,128)(2,1)S(1)} all-gather(f16[32,1024]{1,0:T(8,128)(2,1)S(1)} %convert_element_type.30), channel_id=1, replica_groups=mesh['z'=8,'y'=8,'x'=4,'core'=2] {'z','y'}, dimensions={0}, use_global_device_ids=true | all-gather | bytes 4259840 | tf_op jit(solution)/shard_map/all_gather | solution.py:95
  79.7 1.6 slice_convert_fusion
  81.3 0.0 all-to-all-done.xs
  81.3 0.0 copy-done
  81.3 3.4 %shard_map.83 = (bf16[136,2048]{1,0:T(8,128)(2,1)S(1)}, bf16[136,256]{1,0:T(8,128)(2,1)S(1)}) custom-call(bf16[8,288,256]{2,1,0:T(8,128)(2,1)} %all-to-all-done.xs, bf16[2048,256]{1,0:T(8,128)(2,1)S(1)} %get-tuple-element.32.w_u, bf16[2048,256]{1,0:T(8,128)(2,1)S(1)} %get-tuple-element.31.w_outer, bf16[2048,256]{1,0:T(8,128)(2,1)S(1)} %get-tuple-element.30.w_inner, ...), custom_call_target="tpu_custom_call" | custom-call | flops 1200000000 | bytes 7000000 | tf_op jit(solution)/shard_map/pallas_call | solution.py:155
  84.7 10.6 %collective-permute-start.1 = (bf16[136,2048]{1,0:T(8,128)(2,1)S(1)}, bf16[136,2048]{1,0:T(8,128)(2,1)S(1)}, u32[]{:S(2)}, u32[]{:S(2)}) collective-permute-start(bf16[136,2048]{1,0:T(8,128)(2,1)S(1)} %get-tuple-element.19), channel_id=1, source_target_pairs={{0,1},{1,0},{2,3},{3,2},{4,5},{5,4},{6,7},{7,6},{8,9},{9,8},{10,11... | collective-permute-start | bytes 1671176 | tf_op jit(solution)/shard_map/ppermute | solution.py:99
  95.3 1.8 %shard_map.84 = (bf16[136,2048]{1,0:T(8,128)(2,1)S(1)}, f32[40,2048]{1,0:T(8,128)S(1)}, f32[4,2048]{1,0:T(4,128)S(1)}) custom-call(bf16[136,256]{1,0:T(8,128)(2,1)S(1)} %get-tuple-element.20.rows, bf16[2048,256]{1,0:T(8,128)(2,1)} %get-tuple-element.29.w_out.w, bf16[8,288,256]{2,1,0:T(8,128)(2,1)} %all-to-all-done.xs), custom_call_target="tpu_custom_call" | custom-call | flops 800000000 | bytes 2000000 | tf_op jit(solution)/shard_map/pallas_call | solution.py:198
  97.1 0.0 collective-permute-done.1.got
  97.1 0.3 shard_map.85
  97.4 15.4 %all_to_all.20.got = bf16[4,32,2176]{2,1,0:T(8,128)(2,1)S(1)} all-to-all(bf16[4,32,2176]{2,1,0:T(8,128)(2,1)S(1)} %shard_map.85), channel_id=1, replica_groups=mesh['z'=8,'y'=8,'x'=4,'core'=2] {'x'}, dimensions={0} | all-to-all | bytes 1114112 | tf_op jit(solution)/shard_map/all_to_all | solution.py:101
  112.8 0.3 shard_map.86
  113.1 15.0 %all-gather.6 = f16[256,2048]{1,0:T(8,128)(2,1)S(1)} all-gather(f16[32,2048]{1,0:T(8,128)(2,1)S(1)} %convert_element_type.35), channel_id=1, replica_groups=mesh['z'=8,'y'=8,'x'=4,'core'=2] {'x','core'}, dimensions={0}, use_global_device_ids=true | all-gather | bytes 1179648 | tf_op jit(solution)/shard_map/all_gather | solution.py:103
  128.2 0.1 convert_element_type.36.x
  128.3 0.0 all-gather.4.cloned.1.call-done.w
  128.3 3.5 %shard_map.87 = (bf16[128,2048]{1,0:T(8,128)(2,1)S(1)}, bf16[128,256]{1,0:T(8,128)(2,1)S(1)}) custom-call(bf16[256,2048]{1,0:T(8,128)(2,1)S(1)} %convert_element_type.36.x, bf16[8,2048]{1,0:T(8,128)(2,1)S(1)} %get-tuple-element.25.before, bf16[2048,1024]{1,0:T(8,128)(2,1)} %all-gather.4.cloned.1.call-done.w, f32[3,2,256]{2,1,0:T(2,128)S(1)} %bitcast.5), custom_call_target="tpu_custom_call" | custom-call | flops 1200000000 | bytes 7000000 | tf_op jit(solution)/shard_map/pallas_call | solution.py:307
  131.8 2.1 %collective-permute-start.2 = (bf16[128,2048]{1,0:T(8,128)(2,1)S(1)}, bf16[128,2048]{1,0:T(8,128)(2,1)S(1)}, u32[]{:S(2)}, u32[]{:S(2)}) collective-permute-start(bf16[128,2048]{1,0:T(8,128)(2,1)S(1)} %get-tuple-element.27), channel_id=1, source_target_pairs={{0,1},{1,0},{2,3},{3,2},{4,5},{5,4},{6,7},{7,6},{8,9},{9,8},{10,11... | collective-permute-start | bytes 1572872 | tf_op jit(solution)/shard_map/ppermute | solution.py:106
  133.9 1.7 %shard_map.88 = bf16[128,2048]{1,0:T(8,128)(2,1)S(1)} custom-call(bf16[128,256]{1,0:T(8,128)(2,1)S(1)} %get-tuple-element.28.rows, bf16[2048,1024]{1,0:T(8,128)(2,1)} %all-gather.4.cloned.1.call-done.w), custom_call_target="tpu_custom_call" | custom-call | flops 800000000 | bytes 2000000 | tf_op jit(solution)/shard_map/pallas_call | solution.py:222
  135.6 0.0 collective-permute-done.2
  135.6 0.1 add_convert_fusion
  135.8 11.5 %all_to_all.21.got = bf16[4,32,2048]{2,1,0:T(8,128)(2,1)S(1)} all-to-all(bf16[4,32,2048]{2,1,0:T(8,128)(2,1)S(1)} %bitcast.6), channel_id=1, replica_groups=mesh['z'=8,'y'=8,'x'=4,'core'=2] {'x'}, dimensions={0} | all-to-all | bytes 1048576 | tf_op jit(solution)/shard_map/all_to_all | solution.py:108
  147.3 0.3 shard_map.89
  147.6 9.0 %all_to_all.22 = bf16[8,32,256]{2,1,0:T(8,128)(2,1)S(1)} all-to-all(bf16[8,32,256]{2,1,0:T(8,128)(2,1)S(1)} %shard_map.89), channel_id=1, replica_groups=mesh['z'=8,'y'=8,'x'=4,'core'=2] {'x','core'}, dimensions={0} | all-to-all | bytes 262144 | tf_op jit(solution)/shard_map/all_to_all | solution.py:109
  156.5 0.7 copy.11
  (2 shorter events, 0.0 us)
Async XLA Ops:
  6.5 121.8 %all-gather.4.cloned.1.call-start = ((), (), s32[]{:S(2)}) async-start(), calls=%async_computation.4 | async-start | bytes 4259840 | tf_op jit(solution)/shard_map/all_gather | solution.py:92
  10.0 4.9 %collective-permute-start = (bf16[16,256]{1,0:T(8,128)(2,1)S(1)}, bf16[16,256]{1,0:T(8,128)(2,1)S(1)}, u32[]{:S(2)}, u32[]{:S(2)}) collective-permute-start(bf16[16,256]{1,0:T(8,128)(2,1)S(1)} %slice.15), channel_id=1, source_target_pairs={{0,8},{8,16},{16,24},{24,32},{32,40},{40,48},{48,56},{56,64},{64,7... | collective-permute-start | bytes 24584 | tf_op jit(solution)/shard_map/ppermute | solution.py:90
  15.5 65.8 %all-to-all-start = ((bf16[8,288,256]{2,1,0:T(8,128)(2,1)}), bf16[8,288,256]{2,1,0:T(8,128)(2,1)}, u32[]{:S(2)}, u32[]{:S(2)}) async-start(bf16[8,288,256]{2,1,0:T(8,128)(2,1)} %broadcast_dynamic-update-slice_fusion), calls=%async_computation | async-start | bytes 2359296 | tf_op jit(solution)/shard_map/all_to_all | solution.py:94
  79.7 1.6 %copy-start = (f32[2,3,256]{2,0,1:T(2,128)S(1)}, f32[2,3,256]{2,0,1:T(2,128)}, u32[]{:S(2)}) copy-start(f32[2,3,256]{2,0,1:T(2,128)} %param.12) | copy-start | bytes 18436
  84.7 12.4 %collective-permute-start.1 = (bf16[136,2048]{1,0:T(8,128)(2,1)S(1)}, bf16[136,2048]{1,0:T(8,128)(2,1)S(1)}, u32[]{:S(2)}, u32[]{:S(2)}) collective-permute-start(bf16[136,2048]{1,0:T(8,128)(2,1)S(1)} %get-tuple-element.19), channel_id=1, source_target_pairs={{0,1},{1,0},{2,3},{3,2},{4,5},{5,4},{6,7},{7,6},{8,9},{9,8},{10,11... | collective-permute-start | bytes 1671176 | tf_op jit(solution)/shard_map/ppermute | solution.py:99
  131.8 3.8 %collective-permute-start.2 = (bf16[128,2048]{1,0:T(8,128)(2,1)S(1)}, bf16[128,2048]{1,0:T(8,128)(2,1)S(1)}, u32[]{:S(2)}, u32[]{:S(2)}) collective-permute-start(bf16[128,2048]{1,0:T(8,128)(2,1)S(1)} %get-tuple-element.27), channel_id=1, source_target_pairs={{0,1},{1,0},{2,3},{3,2},{4,5},{5,4},{6,7},{7,6},{8,9},{9,8},{10,11... | collective-permute-start | bytes 1572872 | tf_op jit(solution)/shard_map/ppermute | solution.py:106
Sparse Core Ops, SparseCore 0:
  10.4 91.4 all-gather.3
